TPU v7x, 32 devices: a whole 2x2x4 slice. The times are simulated.
32 devices in a mesh: ep: 16 (over z, y, x), tp: 2 (over core).
Axes of the slice: x: 2, y: 2, z: 4, core: 2. Of those that a mesh axis runs over, the one named last changes fastest.
Arguments:
- tokens: bfloat16 [32, 2048], P('ep'), may hold values from -6 to 6
- head_state: float32 [32, 32, 64, 128], P('ep', 'tp'), may hold values from -4 to 4
- conv_state: bfloat16 [32, 3, 2048], P('ep', None, 'tp'), may hold values from -6 to 6
- conv_proj_state: bfloat16 [32, 3, 2, 512], P('ep', None, None, 'tp'), may hold values from -6 to 6
- first_gain: float32 [2048], replicated, may hold values from 0.1 to 1.9
- gate_weight: bfloat16 [2048, 2048], P('ep', 'tp'), may hold values from -0.125 to 0.125
- inner_weight: bfloat16 [2048, 2048], P('ep', 'tp'), may hold values from -0.125 to 0.125
- write_weight: bfloat16 [2048, 512], P(None, 'tp'), may hold values from -0.125 to 0.125
- read_weight: bfloat16 [2048, 512], P(None, 'tp'), may hold values from -0.125 to 0.125
- step_weight: bfloat16 [2048, 32], P(None, 'tp'), may hold values from -0.125 to 0.125
- conv_kernel: float32 [4, 2048], P(None, 'tp'), may hold values from -3 to 3
- conv_proj_kernel: float32 [4, 2, 512], P(None, None, 'tp'), may hold values from -3 to 3
- step_bias: float32 [32], P('tp'), may hold values from -2 to 1
- log_rate: float32 [32], P('tp'), may hold values from -4.5 to 1.5
- skip_gain: float32 [32], P('tp'), may hold values from 0.5 to 2
- group_gain: float32 [2048], P('tp'), may hold values from 0.1 to 1.9
- out_weight: bfloat16 [2048, 2048], P('tp', 'ep'), may hold values from -0.125 to 0.125
- second_gain: float32 [2048], replicated, may hold values from 0.1 to 1.9
- routes: int32 [32, 4], P('ep'), may hold values from 0 to 15, all different within a row; in each aligned block of 32 rows (0 to 31, 32 to 63, ...) at most 32 rows name the same one
- route_logits: bfloat16 [32, 4], P('ep'), may hold values from -8 to 300
- expert_gate: bfloat16 [16, 2048, 1024], P('ep', None, 'tp'), may hold values from -0.5 to 0.5
- expert_up: bfloat16 [16, 2048, 1024], P('ep', None, 'tp'), may hold values from -0.5 to 0.5
- expert_down: bfloat16 [16, 1024, 2048], P('ep', 'tp'), may hold values from -0.0234375 to 0.0234375
- dense_up: bfloat16 [2048, 4096], P(None, ('ep', 'tp')), may hold values from -0.125 to 0.125
- dense_down: bfloat16 [4096, 2048], P(('ep', 'tp')), may hold values from -0.09375 to 0.09375
- dense_gate: float32 [2048], replicated, may hold values from -0.125 to 0.125
Outputs:
- layer_out: bfloat16 [32, 2048], P(('ep', 'tp'))
- state_out: float32 [32, 32, 64, 128], P('ep', 'tp')
- conv_out: bfloat16 [32, 3, 2048], P('ep', None, 'tp')
- conv_proj_out: bfloat16 [32, 3, 2, 512], P('ep', None, None, 'tp')
Inputs may be any that keep to these rules, and one draw needn't show every extreme that they name: `routes`: each token names 4 different experts; over the whole batch no expert is named by more than 32 rows, a bound that some block reaches.
All inputs are finite; a program needn't handle non-finite values.
Results may differ from a plain program's by a relative error of at most 0.015.
Values may be sent and summed in bfloat16 or wider, within the bound.
A program may use at most 64 MiB of HBM per device.

v0:
```python
import jax
import jax.numpy as jnp
from jax import lax
from jax.sharding import PartitionSpec as P

GROUPS = 4


norm_eps = 1e-05
clamp_limit = 7.0
glu_alpha = 1.702
highest = lax.Precision.HIGHEST


def rms_scale(values, gain_vec):
    return (
        values * lax.rsqrt(jnp.mean(values * values, axis=-1, keepdims=True) + norm_eps) * gain_vec
    )


def clamped_unit(gate_pre, up_pre):
    glu_part = jnp.minimum(gate_pre, clamp_limit)
    lin_part = jnp.clip(up_pre, -clamp_limit, clamp_limit)
    return glu_part * jax.nn.sigmoid(glu_alpha * glu_part) * (lin_part + 1.0)


def state_step(
    inner_proj,
    gate_proj,
    write_proj,
    read_proj,
    step_raw,
    conv_state,
    conv_proj_state,
    conv_kernel,
    conv_proj_kernel,
    step_bias,
    log_rate,
    skip_gain,
    group_gain,
    head_state,
    group_count,
):
    window_inner = jnp.concatenate([conv_state, inner_proj[:, None, :]], axis=1)
    window_proj = jnp.concatenate(
        [conv_proj_state, jnp.stack([write_proj, read_proj], axis=1)[:, None]], axis=1
    )
    conv_inner = jax.nn.silu(jnp.sum(window_inner.astype(jnp.float32) * conv_kernel[None], axis=1))
    conv_proj = jax.nn.silu(
        jnp.sum(window_proj.astype(jnp.float32) * conv_proj_kernel[None], axis=1)
    )
    seq_count, channels = conv_inner.shape
    head_count = step_raw.shape[1]
    head_width = channels // head_count
    state_width = conv_proj.shape[2] // group_count
    per_group = head_count // group_count
    head_input = conv_inner.reshape(seq_count, head_count, head_width)
    write_heads = jnp.repeat(
        conv_proj[:, 0].reshape(seq_count, group_count, state_width), per_group, axis=1
    )
    read_heads = jnp.repeat(
        conv_proj[:, 1].reshape(seq_count, group_count, state_width), per_group, axis=1
    )
    step_size = jax.nn.softplus(step_raw + step_bias)
    decay_rate = jnp.exp(-jnp.exp(log_rate) * step_size)
    state_out = (
        decay_rate[:, :, None, None] * head_state
        + (step_size[:, :, None] * head_input)[:, :, :, None] * write_heads[:, :, None, :]
    )
    read_out = (
        jnp.einsum("shpn,shn->shp", state_out, read_heads, precision=highest)
        + skip_gain[None, :, None] * head_input
    )
    gated_rows = read_out.reshape(seq_count, channels) * jax.nn.silu(gate_proj.astype(jnp.float32))
    grouped = gated_rows.reshape(seq_count, group_count, channels // group_count)
    grouped = grouped * lax.rsqrt(jnp.mean(grouped * grouped, axis=-1, keepdims=True) + norm_eps)
    mixer_rows = (grouped.reshape(seq_count, channels) * group_gain).astype(jnp.bfloat16)
    return (mixer_rows, state_out, window_inner[:, 1:], window_proj[:, 1:])


def local(
    tokens,
    head_state,
    conv_state,
    conv_proj_state,
    first_gain,
    gate_weight,
    inner_weight,
    write_weight,
    read_weight,
    step_weight,
    conv_kernel,
    conv_proj_kernel,
    step_bias,
    log_rate,
    skip_gain,
    group_gain,
    out_weight,
    second_gain,
    routes,
    route_logits,
    expert_gate,
    expert_up,
    expert_down,
    dense_up,
    dense_down,
    dense_gate,
):
    seq_count = tokens.shape[0]
    half_width = gate_weight.shape[1]
    normed_in = rms_scale(tokens.astype(jnp.float32), first_gain).astype(jnp.bfloat16)
    features = lax.all_to_all(normed_in, "ep", split_axis=1, concat_axis=0, tiled=True)
    row_block = features
    both_terms = lax.psum_scatter(
        jnp.concatenate(
            [
                jnp.dot(row_block, gate_weight, preferred_element_type=jnp.float32),
                jnp.dot(row_block, inner_weight, preferred_element_type=jnp.float32),
            ],
            axis=1,
        ),
        "ep",
        scatter_dimension=0,
        tiled=True,
    )
    gate_sum = both_terms[:, :half_width]
    inner_sum = both_terms[:, half_width:]
    gate_proj = gate_sum.astype(jnp.bfloat16)
    inner_proj = inner_sum.astype(jnp.bfloat16)
    write_proj = jnp.dot(normed_in, write_weight, preferred_element_type=jnp.float32).astype(
        jnp.bfloat16
    )
    read_proj = jnp.dot(normed_in, read_weight, preferred_element_type=jnp.float32).astype(
        jnp.bfloat16
    )
    step_raw = jnp.dot(normed_in, step_weight, preferred_element_type=jnp.float32)
    local_groups = GROUPS // lax.axis_size("tp")
    mixer_rows, state_out, conv_out, conv_proj_out = state_step(
        inner_proj,
        gate_proj,
        write_proj,
        read_proj,
        step_raw,
        conv_state,
        conv_proj_state,
        conv_kernel,
        conv_proj_kernel,
        step_bias,
        log_rate,
        skip_gain,
        group_gain,
        head_state,
        local_groups,
    )
    partial_mix = jnp.dot(
        mixer_rows,
        lax.all_gather(out_weight, "ep", axis=1, tiled=True),
        preferred_element_type=jnp.float32,
    )
    mixed = lax.psum(partial_mix, "tp")
    hidden = (tokens.astype(jnp.float32) + mixed).astype(jnp.bfloat16)
    normed_mid = rms_scale(hidden.astype(jnp.float32), second_gain).astype(jnp.bfloat16)
    all_rows, all_routes, all_logits = (
        lax.all_gather(normed_mid, "ep", axis=0, tiled=True),
        lax.all_gather(routes, "ep", axis=0, tiled=True),
        lax.all_gather(route_logits, "ep", axis=0, tiled=True),
    )
    route_gates = jax.nn.softmax(all_logits.astype(jnp.float32), axis=-1)
    my_expert = lax.axis_index("ep")
    route_hits = all_routes == my_expert
    row_weight = jnp.sum(jnp.where(route_hits, route_gates, 0.0), axis=1)
    chosen = jnp.any(route_hits, axis=1)
    slot_index = jnp.cumsum(chosen.astype(jnp.int32)) - 1
    capacity = 4 * seq_count * routes.shape[1]
    slot_ids = jnp.arange(capacity, dtype=jnp.int32)
    picks = (slot_index[None, :] == slot_ids[:, None]) & chosen[None, :]
    picked_rows = jnp.dot(
        picks.astype(jnp.bfloat16), all_rows, preferred_element_type=jnp.float32
    ).astype(jnp.bfloat16)
    activated = clamped_unit(
        jnp.dot(picked_rows, expert_gate[0], preferred_element_type=jnp.float32),
        jnp.dot(picked_rows, expert_up[0], preferred_element_type=jnp.float32),
    ).astype(jnp.bfloat16)
    expert_part = jnp.dot(activated, expert_down[0], preferred_element_type=jnp.float32)
    placed = jnp.where(picks, row_weight[None, :], 0.0)
    dense_weight = jax.nn.sigmoid(
        jnp.dot(all_rows.astype(jnp.float32), dense_gate, precision=highest)
    )
    row_share = seq_count // lax.axis_size("tp")
    row_block = all_rows
    dense_inner = jax.nn.silu(
        jnp.dot(row_block, dense_up, preferred_element_type=jnp.float32)
    ).astype(jnp.bfloat16)
    dense_term = (
        jnp.dot(dense_inner, dense_down, preferred_element_type=jnp.float32) * dense_weight[:, None]
    )
    summed = lax.psum_scatter(
        dense_term + jnp.einsum("cr,cd->rd", placed, expert_part, precision=highest),
        ("ep", "tp"),
        scatter_dimension=0,
        tiled=True,
    )
    own_rows = lax.dynamic_slice_in_dim(hidden, lax.axis_index("tp") * row_share, row_share, 0)
    layer_out = (own_rows.astype(jnp.float32) + summed).astype(jnp.bfloat16)
    return (layer_out, state_out, conv_out, conv_proj_out)


def solution(mesh):
    placed = (
        P("ep", None),
        P("ep", "tp", None, None),
        P("ep", None, "tp"),
        P("ep", None, None, "tp"),
        P(),
        P("ep", "tp"),
        P("ep", "tp"),
        P(None, "tp"),
        P(None, "tp"),
        P(None, "tp"),
        P(None, "tp"),
        P(None, None, "tp"),
        P("tp"),
        P("tp"),
        P("tp"),
        P("tp"),
        P("tp", "ep"),
        P(),
        P("ep", None),
        P("ep", None),
        P("ep", None, "tp"),
        P("ep", None, "tp"),
        P("ep", "tp", None),
        P(None, ("ep", "tp")),
        P(("ep", "tp"), None),
        P(),
    )
    return jax.shard_map(
        local,
        mesh=mesh,
        in_specs=placed,
        out_specs=(
            P(("ep", "tp"), None),
            P("ep", "tp", None, None),
            P("ep", None, "tp"),
            P("ep", None, None, "tp"),
        ),
        check_vma=False,
    )
```

profile of v0, /device:TPU:0, one launch (start us, length us, event | category | flops | bytes accessed | tf_op | source)
XLA Modules:
  0.0 366.6 jit_solution(6671447801654428181)
XLA Ops:
  7.2 0.0 copy-start
  7.2 0.0 copy-start.18
  7.2 0.0 copy-start.5
  7.2 0.0 copy-start.6
  7.3 0.0 all-gather.5.cloned.1.call-start
  7.3 0.7 all-gather.5.cloned.1.call-update
  8.0 0.9 fusion.43
  8.9 1.4 fusion.107
  10.3 8.3 %all-to-all-start = ((bf16[2,16,128]{2,0,1:T(2,128)(2,1)}), bf16[2,16,128]{2,0,1:T(2,128)(2,1)S(1)}, u32[]{:S(2)}, u32[]{:S(2)}) async-start(bf16[2,16,128]{2,0,1:T(2,128)(2,1)} %fusion.107), calls=%async_computation | async-start | bytes 16384 | tf_op jit(solution)/shard_map/all_to_all | solution.py:112
  18.7 0.0 all-reduce.5.cloned.1.call-start
  18.7 41.6 %all-gather.1 = s32[16,2,4]{2,1,0:T(2,128)S(1)} all-gather(s32[1,2,4]{2,1,0:T(2,128)} %bitcast.98), channel_id=1, replica_groups=mesh['ep'=16,'tp'=2] {'ep'}, dimensions={0}, use_global_device_ids=true | all-gather | bytes 544 | tf_op jit(solution)/shard_map/all_gather | solution.py:165
  60.4 0.4 fusion.77
  60.7 0.1 reshape.124
  60.8 0.1 copy.41
  60.9 36.8 %all-gather.2 = bf16[16,2,4]{2,1,0:T(2,128)(2,1)S(1)} all-gather(bf16[1,2,4]{2,1,0:T(2,128)(2,1)} %bitcast.99), channel_id=1, replica_groups=mesh['ep'=16,'tp'=2] {'ep'}, dimensions={0}, use_global_device_ids=true | all-gather | bytes 272 | tf_op jit(solution)/shard_map/all_gather | solution.py:166
  97.7 0.1 reduce.1
  97.8 0.1 reshape.123
  97.9 0.1 copy.43
  98.0 0.1 copy.46
  98.1 0.1 reduce-window.8
  98.2 1.5 fusion.24
  99.7 1.5 fusion.25
  101.3 0.1 add_reduce_fusion
  101.4 0.0 copy-done.10
  101.5 0.0 copy-done.16
  101.6 0.2 multiply_exponential_fusion
  101.8 0.6 dynamic-slice
  103.1 0.0 all-to-all-done
  103.1 0.2 fusion.82
  103.3 0.2 fusion.83
  103.4 0.0 copy-start.13
  103.4 0.0 copy-start.12
  103.5 75.9 %all-reduce.6 = bf16[32,2048]{1,0:T(8,128)(2,1)S(1)} all-reduce(f32[32,2048]{1,0:T(8,128)S(1)} %pad_maximum_fusion), channel_id=2, replica_groups=mesh['ep'=16,'tp'=2] {'ep'}, use_global_device_ids=true, to_apply=%region_1.0.clone | all-reduce | flops 65536 | bytes 393216
  179.4 0.1 reduce_sum.67
  179.5 0.1 broadcast_multiply_fusion
  179.6 1.6 multiply_add_fusion
  181.2 0.0 copy-start.1
  181.2 1.7 fusion.84
  183.0 0.1 multiply_add_fusion.1
  183.1 0.1 reshape.111
  183.2 0.1 reduce_sum.69
  183.3 0.1 broadcast_bitcast_fusion.1
  183.4 0.0 all-gather.5.cloned.1.call-done
  183.4 0.0 copy-start.9
  183.4 0.0 copy-start.15
  183.4 2.8 fusion.65
  186.3 3.4 psum.7
  189.6 0.1 fusion.40
  189.8 0.1 fusion.62
  189.9 36.5 %all-gather = bf16[16,2,2048]{2,1,0:T(2,128)(2,1)S(1)} all-gather(bf16[1,2,2048]{2,1,0:T(2,128)(2,1)S(1)} %fusion.62), channel_id=1, replica_groups=mesh['ep'=16,'tp'=2] {'ep'}, dimensions={0}, use_global_device_ids=true | all-gather | bytes 139264 | tf_op jit(solution)/shard_map/all_gather | solution.py:164
  226.3 0.1 reshape.114
  226.4 0.2 convolution_convert_fusion
  226.6 0.2 fusion.29
  226.7 2.1 fusion.7
  228.8 0.0 copy-done
  228.9 0.0 copy-start.2
  228.9 2.5 fusion.1
  231.4 0.4 fusion.47
  231.9 2.2 fusion
  234.0 0.0 all-reduce.5.cloned.1.call-update
  234.1 0.6 slice.32
  234.7 0.6 fusion.52
  235.3 123.0 %all-reduce.5.cloned.1.call-done = f32[32,2048]{1,0:T(8,128)} async-done(((f32[32,2048]{1,0:T(8,128)}), f32[32,2048]{1,0:T(8,128)}) %all-reduce.5.cloned.1.call-update) | async-done | bytes 262160
  358.3 1.5 fusion.56
  (48 shorter events, 0.4 us)
Async XLA Ops:
  7.2 221.7 %copy-start = (bf16[1,512,2048]{2,1,0:T(8,128)(2,1)S(1)}, bf16[1,512,2048]{2,1,0:T(8,128)(2,1)}, u32[]{:S(2)}) copy-start(bf16[1,512,2048]{2,1,0:T(8,128)(2,1)} %param.48) | copy-start | bytes 6291460
  7.2 94.7 %copy-start.18 = (u32[32]{0:T(128)S(1)}, u32[32]{0:T(128)}, u32[]{:S(2)}) copy-start(u32[32]{0:T(128)} %constant.66) | copy-start | bytes 388
  7.2 94.4 %copy-start.5 = (bf16[2,2048]{1,0:T(2,128)(2,1)S(1)}, bf16[2,2048]{1,0:T(2,128)(2,1)}, u32[]{:S(2)}) copy-start(bf16[2,2048]{1,0:T(2,128)(2,1)} %param.26) | copy-start | bytes 24580
  7.2 94.4 %copy-start.6 = (f32[2048]{0:T(1024)S(1)}, f32[2048]{0:T(1024)}, u32[]{:S(2)}) copy-start(f32[2048]{0:T(1024)} %param.30) | copy-start | bytes 24580
  7.2 94.1 %copy-start.11 = (bf16[2,3,2,256]{3,2,1,0:T(2,128)(2,1)S(1)}, bf16[2,3,2,256]{3,2,1,0:T(2,128)(2,1)}, u32[]{:S(2)}) copy-start(bf16[2,3,2,256]{3,2,1,0:T(2,128)(2,1)} %param.29) | copy-start | bytes 18436
  7.2 94.2 %copy-start.10 = (f32[4,2,256]{2,1,0:T(2,128)S(1)}, f32[4,2,256]{2,1,0:T(2,128)}, u32[]{:S(2)}) copy-start(f32[4,2,256]{2,1,0:T(2,128)} %param.37) | copy-start | bytes 24580
  7.2 94.2 %copy-start.16 = (f32[16]{0:T(128)S(1)}, f32[16]{0:T(128)}, u32[]{:S(2)}) copy-start(f32[16]{0:T(128)} %param.39) | copy-start | bytes 196
  7.2 94.3 %copy-start.14 = (bf16[2048,16]{0,1:T(8,128)(2,1)S(1)}, bf16[2048,16]{0,1:T(8,128)(2,1)}, u32[]{:S(2)}) copy-start(bf16[2048,16]{0,1:T(8,128)(2,1)} %param.35) | copy-start | bytes 196612
  7.3 94.3 %copy-start.17 = (f32[16]{0:T(128)S(1)}, f32[16]{0:T(128)}, u32[]{:S(2)}) copy-start(f32[16]{0:T(128)} %param.38) | copy-start | bytes 196
  7.3 95.8 %copy-start.3 = (bf16[128,1024]{1,0:T(8,128)(2,1)S(1)}, bf16[128,1024]{1,0:T(8,128)(2,1)}, u32[]{:S(2)}) copy-start(bf16[128,1024]{1,0:T(8,128)(2,1)} %param.31) | copy-start | bytes 786436
  7.3 96.0 %copy-start.4 = (bf16[128,1024]{1,0:T(8,128)(2,1)S(1)}, bf16[128,1024]{1,0:T(8,128)(2,1)}, u32[]{:S(2)}) copy-start(bf16[128,1024]{1,0:T(8,128)(2,1)} %param.32) | copy-start | bytes 786436
  7.3 176.1 %all-gather.5.cloned.1.call-start = ((), (), s32[]{:S(2)}) async-start(), calls=%async_computation.1 | async-start | bytes 4456448 | tf_op jit(solution)/shard_map/all_gather | solution.py:157
  10.3 92.8 %all-to-all-start = ((bf16[2,16,128]{2,0,1:T(2,128)(2,1)}), bf16[2,16,128]{2,0,1:T(2,128)(2,1)S(1)}, u32[]{:S(2)}, u32[]{:S(2)}) async-start(bf16[2,16,128]{2,0,1:T(2,128)(2,1)} %fusion.107), calls=%async_computation | async-start | bytes 16384 | tf_op jit(solution)/shard_map/all_to_all | solution.py:112
  18.7 339.6 %all-reduce.5.cloned.1.call-start = ((), (), s32[]{:S(2)}) async-start(), calls=%async_computation.2 | async-start | bytes 524288
  98.0 81.4 %copy-start.7 = (bf16[2,3,1024]{2,0,1:T(2,128)(2,1)S(1)}, bf16[2,3,1024]{2,0,1:T(2,128)(2,1)}, u32[]{:S(2)}) copy-start(bf16[2,3,1024]{2,0,1:T(2,128)(2,1)} %param.28) | copy-start | bytes 36868
  98.0 81.4 %copy-start.8 = (f32[4,1024]{1,0:T(4,128)S(1)}, f32[4,1024]{1,0:T(4,128)}, u32[]{:S(2)}) copy-start(f32[4,1024]{1,0:T(4,128)} %param.36) | copy-start | bytes 49156
  103.4 79.5 %copy-start.13 = (f32[16]{0:T(128)S(1)}, f32[16]{0:T(128)}, u32[]{:S(2)}) copy-start(f32[16]{0:T(128)} %param.40) | copy-start | bytes 196
  103.4 80.0 %copy-start.12 = (f32[1024]{0:T(1024)S(1)}, f32[1024]{0:T(1024)}, u32[]{:S(2)}) copy-start(f32[1024]{0:T(1024)} %param.41) | copy-start | bytes 12292
  181.2 5.1 %copy-start.1 = (f32[2,16,64,128]{3,2,1,0:T(8,128)}, f32[2,16,64,128]{3,2,1,0:T(8,128)S(1)}, u32[]{:S(2)}) copy-start(f32[2,16,64,128]{3,2,1,0:T(8,128)S(1)} %multiply_add_fusion) | copy-start | bytes 3145732
  183.4 6.4 %copy-start.9 = (f32[2048]{0:T(1024)S(1)}, f32[2048]{0:T(1024)}, u32[]{:S(2)}) copy-start(f32[2048]{0:T(1024)} %param.43) | copy-start | bytes 24580
  183.4 43.1 %copy-start.15 = (f32[2048]{0:T(1024)S(1)}, f32[2048]{0:T(1024)}, u32[]{:S(2)}) copy-start(f32[2048]{0:T(1024)} %param.51) | copy-start | bytes 24580
  228.9 3.0 copy-start.2
Sparse Core Ops, SparseCore 0:
  10.8 92.4 all-gather.4
  234.2 124.0 all-reduce.4
where the time goes:
time: 367 us
  blocking collectives  194 us (53%)
  waiting for transfers between devices  124 us (34%)
  matrix products  15.7 us (4%)
  between operations  15.2 us (4%)
  starting transfers between devices  8.42 us (2%)
  other arithmetic  7.27 us (2%)
    unnamed x3, waiting for transfers between devices  124 us
    unnamed x1, blocking collectives  75.9 us
    all_gather x1, blocking collectives, local(): lax.all_gather(routes, 'ep', axis=0, tiled=True)  41.6 us
    all_gather x1, blocking collectives, local(): lax.all_gather(route_logits, 'ep', axis=0, tiled=True)  36.8 us
    all_gather x1, blocking collectives, local(): lax.all_gather(normed_mid, 'ep', axis=0, tiled=True)  36.5 us
    all_to_all x1, starting transfers between devices, local(): lax.all_to_all(normed_in, 'ep', split_axis=1, concat_axis=0, tiled=True)  8.34 us
  transfers between devices with their start and end apart: 3, of which 1 were waited for; matrix products, arithmetic and copies ran while one was open for 4% of the time, Pallas kernels for 0%

commit v1 on v0

--- a/solution.py
+++ b/solution.py
@@ -1,6 +1,11 @@
+import functools
+import types
+
 import jax
 import jax.numpy as jnp
 from jax import lax
+from jax.experimental import pallas as pl
+from jax.experimental.pallas import tpu as pltpu
 from jax.sharding import PartitionSpec as P
 
 GROUPS = 4
@@ -205,7 +210,496 @@
     return (layer_out, state_out, conv_out, conv_proj_out)
 
 
+LANES = 128
+MESH = pl.DeviceIdType.MESH
+F32 = jnp.float32
+BF16 = jnp.bfloat16
+
+
+def silu(x):
+    return x * jax.nn.sigmoid(x)
+
+
+def dot(a, b):
+    return jnp.dot(a, b, preferred_element_type=F32)
+
+
+def lanes_of(ref, start, count, stride, pieces):
+    return jnp.concatenate(
+        [ref[pl.ds(start + j, count, stride=stride), :] for j in range(pieces)], axis=1
+    )
+
+
+def layer_kernel(
+    n,
+    nc,
+    names,
+    scratch_names,
+    *refs,
+):
+    r = types.SimpleNamespace(**dict(zip(names + scratch_names, refs)))
+    me = lax.axis_index("ep")
+    core = lax.axis_index("tp")
+    q = r.tokens.shape[0]
+    width = r.tokens.shape[1]
+    half = r.gate_v.shape[1]
+    chunks = half // LANES
+    wide_chunks = width // LANES
+    rows = n * q
+    slot1 = r.send1.shape[0] // n
+    slot2 = 2 * q * chunks
+    slot3 = q * chunks
+    slot6 = wide_chunks
+    heads = r.step_bias.shape[1]
+    head_width = half // heads
+    state_width = r.hs.shape[2]
+    groups = r.write_v.shape[1] // state_width
+    group_width = half // groups
+    topk = r.routes.shape[1]
+
+    barrier = pltpu.get_barrier_semaphore()
+
+    def greet(step, _):
+        other = lax.rem(me * nc + core + step, n * nc)
+        pl.semaphore_signal(
+            barrier, inc=1, device_id=(other // nc, lax.rem(other, nc)), device_id_type=MESH
+        )
+        return 0
+
+    lax.fori_loop(1, n * nc, greet, 0)
+
+    order = (
+        (r.gate_weight, r.gate_v),
+        (r.inner_weight, r.inner_v),
+        (r.write_weight, r.write_v),
+        (r.read_weight, r.read_v),
+        (r.step_weight, r.step_v),
+        (r.head_state, r.hs),
+        (r.out_weight, r.out_v),
+        (r.expert_gate, r.eg_v),
+        (r.expert_up, r.eu_v),
+        (r.dense_up, r.du_v),
+        (r.expert_down, r.ed_v),
+        (r.dense_down, r.dd_v),
+    )
+    loads = [
+        pltpu.make_async_copy(src, dst, r.load_sem.at[i]) for i, (src, dst) in enumerate(order)
+    ]
+    for load in loads:
+        load.start()
+    (
+        gate_load,
+        inner_load,
+        write_load,
+        read_load,
+        step_load,
+        state_load,
+        out_load,
+        expert_gate_load,
+        expert_up_load,
+        dense_up_load,
+        expert_down_load,
+        dense_down_load,
+    ) = loads
+
+    def all_to_all(phase, send, recv, slot, same=False):
+        def one(step, _):
+            peer = lax.rem(me + step, n)
+            src = send if same else send.at[pl.ds(pl.multiple_of(peer * slot, slot), slot)]
+            pltpu.make_async_remote_copy(
+                src_ref=src,
+                dst_ref=recv.at[pl.ds(pl.multiple_of(me * slot, slot), slot)],
+                send_sem=r.send_sem.at[phase],
+                recv_sem=r.recv_sem.at[phase],
+                device_id=(peer, core),
+                device_id_type=MESH,
+            ).start()
+            return 0
+
+        lax.fori_loop(1, n, one, 0)
+
+    def drain(sem, buffer, count):
+        part = buffer.at[pl.ds(0, count)]
+        pltpu.make_async_copy(part, part, sem).wait()
+
+    def take(phase, send, recv, slot, same=False):
+        drain(r.recv_sem.at[phase], recv, (n - 1) * slot)
+        mine = pl.ds(pl.multiple_of(me * slot, slot), slot)
+        recv[mine, :] = send[...] if same else send[mine, :]
+
+    x = r.tokens[...].astype(F32)
+    normed = rms_scale(x, r.first_gain[...]).astype(BF16).astype(F32)
+    send1 = r.send1
+    send1[...] = jnp.zeros_like(send1)
+    chosen = r.routes[...].astype(F32)
+    scores = r.route_logits[...].astype(F32)
+    for e in range(n):
+        at, cut = e * slot1, slice(e * LANES, (e + 1) * LANES)
+        send1[at : at + q, :] = normed[:, cut]
+        send1[at + q : at + 2 * q, :] = x[:, cut]
+        send1[at + 2 * q : at + 3 * q, 0:topk] = chosen
+        send1[at + 3 * q : at + 4 * q, 0:topk] = scores
+    pl.semaphore_wait(barrier, n * nc - 1)
+    all_to_all(0, send1, r.recv1, slot1)
+
+    own = r.own_rows
+    own[...] = jnp.zeros_like(own)
+    own[0:q, :] = normed
+    own_b = own[...].astype(BF16)
+    gate_load.wait()
+    inner_load.wait()
+    write_load.wait()
+    read_load.wait()
+    step_load.wait()
+    write_proj = dot(own_b, r.write_v[...])[0:q].astype(BF16)
+    read_proj = dot(own_b, r.read_v[...])[0:q].astype(BF16)
+    step_raw = dot(own_b, r.step_v[...])[0:q]
+
+    take(0, send1, r.recv1, slot1)
+    recv1 = r.recv1
+
+    def gathered(offset):
+        return jnp.concatenate(
+            [recv1[pl.ds(offset + s, n, stride=slot1), :] for s in range(q)], axis=0
+        )
+
+    features = gathered(0).astype(BF16)
+    pack2 = r.pack2
+    for g, weight in enumerate((r.gate_v, r.inner_v)):
+        part = dot(features, weight[...])
+        for s in range(q):
+            for j in range(chunks):
+                pack2[pl.ds((s * 2 + g) * chunks + j, n, stride=slot2), :] = part[
+                    s * n : (s + 1) * n, j * LANES : (j + 1) * LANES
+                ]
+    r.send2[...] = pack2[...].astype(BF16)
+    all_to_all(1, r.send2, r.recv2, slot2)
+
+    r.proj_out[:, 0 : groups * state_width] = write_proj
+    r.proj_out[:, groups * state_width :] = read_proj
+    proj_tap = r.conv_proj_kernel[r.conv_proj_kernel.shape[0] - 1]
+    gs = groups * state_width
+    write = silu(r.proj_part[:, 0:gs] + write_proj.astype(F32) * proj_tap[0:1])
+    read = silu(r.proj_part[:, gs:] + read_proj.astype(F32) * proj_tap[1:2])
+    pre = step_raw + r.step_bias[...]
+    step_size = jnp.maximum(pre, 0.0) + jnp.log1p(jnp.exp(-jnp.abs(pre)))
+    decay = jnp.exp(-jnp.exp(r.log_rate[...]) * step_size)
+    small = r.small
+    small[...] = jnp.zeros_like(small)
+    small[0:q, :] = step_size
+    small[q : 2 * q, :] = decay
+    small[2 * q : 2 * q + 1, :] = r.skip_gain[...]
+    spread = (
+        lax.broadcasted_iota(jnp.int32, (heads, half), 1) // head_width
+        == lax.broadcasted_iota(jnp.int32, (heads, half), 0)
+    ).astype(F32)
+    by_channel = jnp.dot(small[...], spread, precision=highest, preferred_element_type=F32)
+    step_rows, decay_rows = by_channel[0:q], by_channel[q : 2 * q]
+    skip_rows = by_channel[2 * q : 2 * q + 1]
+    reads = r.reads
+    reads[...] = jnp.zeros_like(reads)
+    reads[0:q, :] = read
+    state_load.wait()
+    old_read = r.old_read
+    write_read = []
+    for g in range(groups):
+        lane = slice(g * state_width, (g + 1) * state_width)
+        span = slice(g * group_width, (g + 1) * group_width)
+        write_read.append(
+            jnp.broadcast_to(
+                jnp.sum(write[:, lane] * read[:, lane], axis=1, keepdims=True), (q, group_width)
+            )
+        )
+        for s in range(q):
+            old_read[s : s + 1, span] = lax.dot_general(
+                reads[:, lane],
+                r.hs[s, span, :],
+                (((1,), (1,)), ((), ())),
+                precision=highest,
+                preferred_element_type=F32,
+            )[s : s + 1]
+    carried = decay_rows * old_read[0:q, :]
+    direct = step_rows * jnp.concatenate(write_read, axis=1) + skip_rows
+
+    all_routes, all_scores = gathered(2 * q), gathered(3 * q)
+    real = lax.broadcasted_iota(jnp.int32, (rows, LANES), 1) < topk
+    top = jnp.max(jnp.where(real, all_scores, -jnp.inf), axis=1, keepdims=True)
+    raised = jnp.where(real, jnp.exp(jnp.where(real, all_scores - top, 0.0)), 0.0)
+    gates = raised / jnp.sum(raised, axis=1, keepdims=True)
+    hits = real & (all_routes == me.astype(F32))
+    row_weight = jnp.sum(jnp.where(hits, gates, 0.0), axis=1, keepdims=True)
+
+    take(1, r.send2, r.recv2, slot2)
+    total = r.recv2[0:slot2, :].astype(F32)
+    for e in range(1, n):
+        total += r.recv2[e * slot2 : (e + 1) * slot2, :].astype(F32)
+    r.sum2[...] = total
+    gate_proj = lanes_of(r.sum2, 0, q, 2 * chunks, chunks).astype(BF16).astype(F32)
+    inner_proj = lanes_of(r.sum2, chunks, q, 2 * chunks, chunks).astype(BF16)
+    last_tap = r.conv_kernel.shape[0] - 1
+    taps = r.conv_kernel[last_tap : last_tap + 1, :]
+    conv_inner = silu(r.inner_part[...] + inner_proj.astype(F32) * taps)
+    gated = (carried + direct * conv_inner) * silu(gate_proj)
+    normal = []
+    for g in range(groups):
+        piece = gated[:, g * group_width : (g + 1) * group_width]
+        normal.append(
+            piece * lax.rsqrt(jnp.mean(piece * piece, axis=1, keepdims=True) + norm_eps)
+        )
+    mixer = jnp.concatenate(normal, axis=1) * r.group_gain[...]
+    for j in range(chunks):
+        r.pack3[pl.ds(j, q, stride=chunks), :] = mixer[:, j * LANES : (j + 1) * LANES]
+    r.send3[...] = r.pack3[...].astype(BF16)
+    all_to_all(2, r.send3, r.recv3, slot3, same=True)
+
+    r.inner_out[...] = inner_proj
+    turn = r.turn
+    turn[...] = jnp.zeros_like(turn)
+    turn[0:q, :] = decay_rows
+    turn[q : 2 * q, :] = step_rows * conv_inner
+    columns = jnp.transpose(turn[...])
+    for s in range(q):
+        for k in range(chunks):
+            span = slice(k * LANES, (k + 1) * LANES)
+            g = k * LANES // group_width
+            r.hs[s, span, :] = (
+                columns[span, s : s + 1] * r.hs[s, span, :]
+                + columns[span, q + s : q + s + 1]
+                * write[s : s + 1, g * state_width : (g + 1) * state_width]
+            )
+    store = pltpu.make_async_copy(r.hs, r.state_out, r.load_sem.at[len(order)])
+    store.start()
+    raw_block = gathered(q)
+    out_load.wait()
+
+    take(2, r.send3, r.recv3, slot3, same=True)
+    r.wide3[...] = r.recv3[...].astype(F32)
+    all_mixer = jnp.concatenate(
+        [lanes_of(r.wide3, s * chunks, n, slot3, chunks) for s in range(q)], axis=0
+    ).astype(BF16)
+    part = dot(all_mixer, r.out_v[...])
+    r.send4[...] = part
+    swap = pltpu.make_async_remote_copy(
+        src_ref=r.send4,
+        dst_ref=r.recv4,
+        send_sem=r.send_sem.at[3],
+        recv_sem=r.recv_sem.at[3],
+        device_id=(me, lax.rem(core + 1, nc)),
+        device_id_type=MESH,
+    )
+    swap.start()
+    swap.wait_recv()
+    r.send5[...] = (raw_block + (part + r.recv4[...])).astype(BF16)
+    all_to_all(4, r.send5, r.recv5, rows, same=True)
+    expert_gate_load.wait()
+    expert_up_load.wait()
+    dense_up_load.wait()
+    take(4, r.send5, r.recv5, rows, same=True)
+    hidden = jnp.concatenate(
+        [r.recv5[e * rows : (e + 1) * rows, :] for e in range(n)], axis=1
+    ).astype(F32)
+    r.hidden[...] = hidden
+    mid = rms_scale(hidden, r.second_gain[...]).astype(BF16)
+    dense_inner = silu(dot(mid, r.du_v[...])).astype(BF16)
+    activated = clamped_unit(dot(mid, r.eg_v[...]), dot(mid, r.eu_v[...])).astype(BF16)
+    dense_weight = jax.nn.sigmoid(
+        jnp.sum(mid.astype(F32) * r.dense_gate[...], axis=1, keepdims=True)
+    )
+    expert_down_load.wait()
+    dense_down_load.wait()
+    cuts = 4
+    for c in range(cuts):
+        span = slice(c * width // cuts, (c + 1) * width // cuts)
+        term = dot(activated, r.ed_v[:, span]) * row_weight
+        term += dot(dense_inner, r.dd_v[:, span]) * dense_weight
+        for j in range(wide_chunks // cuts):
+            r.pack6[pl.ds(c * wide_chunks // cuts + j, rows, stride=slot6), :] = term[
+                :, j * LANES : (j + 1) * LANES
+            ]
+    r.send6[...] = r.pack6[...].astype(BF16)
+    mine = me * nc + core
+
+    def one(step, _):
+        other = lax.rem(mine + step, n * nc)
+        peer, peer_core = other // nc, lax.rem(other, nc)
+        pltpu.make_async_remote_copy(
+            src_ref=r.send6.at[
+                pl.ds(pl.multiple_of((peer_core * n + peer) * slot6, slot6), slot6)
+            ],
+            dst_ref=r.recv6.at[pl.ds(pl.multiple_of(mine * slot6, slot6), slot6)],
+            send_sem=r.send_sem.at[5],
+            recv_sem=r.recv_sem.at[5],
+            device_id=(peer, peer_core),
+            device_id_type=MESH,
+        ).start()
+        return 0
+
+    lax.fori_loop(1, n * nc, one, 0)
+    own_row = r.hidden[pl.ds(core * n + me, 1), :]
+    drain(r.recv_sem.at[5], r.recv6, (n * nc - 1) * slot6)
+    r.recv6[pl.ds(pl.multiple_of(mine * slot6, slot6), slot6), :] = r.send6[
+        pl.ds(pl.multiple_of((core * n + me) * slot6, slot6), slot6), :
+    ]
+    total = r.recv6[0:slot6, :].astype(F32)
+    for e in range(1, n * nc):
+        total += r.recv6[e * slot6 : (e + 1) * slot6, :].astype(F32)
+    r.sum6[...] = total
+    summed = jnp.concatenate([r.sum6[j : j + 1, :] for j in range(wide_chunks)], axis=1)
+    r.layer_out[...] = (own_row + summed).astype(BF16)
+
+    store.wait()
+    drain(r.send_sem.at[0], send1, (n - 1) * slot1)
+    drain(r.send_sem.at[1], r.send2, (n - 1) * slot2)
+    drain(r.send_sem.at[2], r.recv3, (n - 1) * slot3)
+    swap.wait_send()
+    drain(r.send_sem.at[4], r.recv5, (n - 1) * rows)
+    drain(r.send_sem.at[5], r.send6, (n * nc - 1) * slot6)
+
+
+def fused_local(
+    n,
+    nc,
+    tokens,
+    head_state,
+    conv_state,
+    conv_proj_state,
+    first_gain,
+    gate_weight,
+    inner_weight,
+    write_weight,
+    read_weight,
+    step_weight,
+    conv_kernel,
+    conv_proj_kernel,
+    step_bias,
+    log_rate,
+    skip_gain,
+    group_gain,
+    out_weight,
+    second_gain,
+    routes,
+    route_logits,
+    expert_gate,
+    expert_up,
+    expert_down,
+    dense_up,
+    dense_down,
+    dense_gate,
+):
+    q, width = tokens.shape
+    half = gate_weight.shape[1]
+    rows = n * q
+    chunks, wide_chunks = half // LANES, width // LANES
+    gs = write_weight.shape[1]
+    heads, state_width = head_state.shape[1], head_state.shape[3]
+    taps = conv_kernel.shape[0]
+    inner_part = jnp.sum(conv_state.astype(F32) * conv_kernel[None, : taps - 1], axis=1)
+    proj_part = jnp.sum(
+        conv_proj_state.astype(F32) * conv_proj_kernel[None, : taps - 1], axis=1
+    ).reshape(q, 2 * gs)
+    small_in = dict(
+        tokens=tokens,
+        first_gain=first_gain[None],
+        inner_part=inner_part,
+        proj_part=proj_part,
+        conv_kernel=conv_kernel,
+        conv_proj_kernel=conv_proj_kernel,
+        step_bias=step_bias[None],
+        log_rate=log_rate[None],
+        skip_gain=skip_gain[None],
+        group_gain=group_gain[None],
+        second_gain=second_gain[None],
+        routes=routes,
+        route_logits=route_logits,
+        dense_gate=dense_gate[None],
+    )
+    big_in = dict(
+        head_state=head_state.reshape(q, half, state_width),
+        gate_weight=gate_weight,
+        inner_weight=inner_weight,
+        write_weight=write_weight,
+        read_weight=read_weight,
+        step_weight=step_weight,
+        out_weight=out_weight,
+        expert_gate=expert_gate[0],
+        expert_up=expert_up[0],
+        expert_down=expert_down[0],
+        dense_up=dense_up,
+        dense_down=dense_down,
+    )
+    outs = dict(
+        layer_out=jax.ShapeDtypeStruct((q // nc, width), BF16),
+        state_out=jax.ShapeDtypeStruct((q, half, state_width), F32),
+        inner_out=jax.ShapeDtypeStruct((q, half), BF16),
+        proj_out=jax.ShapeDtypeStruct((q, 2 * gs), BF16),
+    )
+    slot1 = -(-4 * q // 8) * 8
+    slot2, slot3, slot6 = 2 * q * chunks, q * chunks, wide_chunks
+    small_rows = -(-(2 * q + 1) // 8) * 8
+    vmem = pltpu.VMEM
+    scratch = dict(
+        gate_v=vmem(gate_weight.shape, BF16),
+        inner_v=vmem(inner_weight.shape, BF16),
+        write_v=vmem(write_weight.shape, BF16),
+        read_v=vmem(read_weight.shape, BF16),
+        step_v=vmem(step_weight.shape, BF16),
+        hs=vmem((q, half, state_width), F32),
+        out_v=vmem(out_weight.shape, BF16),
+        eg_v=vmem(expert_gate.shape[1:], BF16),
+        eu_v=vmem(expert_up.shape[1:], BF16),
+        du_v=vmem(dense_up.shape, BF16),
+        ed_v=vmem(expert_down.shape[1:], BF16),
+        dd_v=vmem(dense_down.shape, BF16),
+        send1=vmem((n * slot1, LANES), F32),
+        recv1=vmem((n * slot1, LANES), F32),
+        own_rows=vmem((16, width), F32),
+        pack2=vmem((n * slot2, LANES), F32),
+        send2=vmem((n * slot2, LANES), BF16),
+        recv2=vmem((n * slot2, LANES), BF16),
+        sum2=vmem((slot2, LANES), F32),
+        small=vmem((small_rows, heads), F32),
+        reads=vmem((8, gs), F32),
+        old_read=vmem((8, half), F32),
+        pack3=vmem((slot3, LANES), F32),
+        send3=vmem((slot3, LANES), BF16),
+        recv3=vmem((n * slot3, LANES), BF16),
+        wide3=vmem((n * slot3, LANES), F32),
+        turn=vmem((8, half), F32),
+        send4=vmem((rows, LANES), F32),
+        recv4=vmem((rows, LANES), F32),
+        send5=vmem((rows, LANES), BF16),
+        recv5=vmem((n * rows, LANES), BF16),
+        hidden=vmem((rows, width), F32),
+        pack6=vmem((rows * slot6, LANES), F32),
+        send6=vmem((rows * slot6, LANES), BF16),
+        recv6=vmem((n * nc * slot6, LANES), BF16),
+        sum6=vmem((slot6, LANES), F32),
+        load_sem=pltpu.SemaphoreType.DMA((13,)),
+        send_sem=pltpu.SemaphoreType.DMA((6,)),
+        recv_sem=pltpu.SemaphoreType.DMA((6,)),
+    )
+    in_vmem = pl.BlockSpec(memory_space=pltpu.VMEM)
+    anywhere = pl.BlockSpec(memory_space=pl.ANY)
+    names = tuple(small_in) + tuple(big_in) + tuple(outs)
+    layer_out, state_out, inner_out, proj_out = pl.pallas_call(
+        functools.partial(layer_kernel, n, nc, names, tuple(scratch)),
+        out_shape=tuple(outs.values()),
+        in_specs=[in_vmem] * len(small_in) + [anywhere] * len(big_in),
+        out_specs=(in_vmem, anywhere, in_vmem, in_vmem),
+        scratch_shapes=list(scratch.values()),
+        compiler_params=pltpu.CompilerParams(
+            collective_id=0, has_side_effects=True, vmem_limit_bytes=60 * 1024 * 1024
+        ),
+    )(*small_in.values(), *big_in.values())
+    conv_out = jnp.concatenate([conv_state[:, 1:], inner_out[:, None]], axis=1)
+    conv_proj_out = jnp.concatenate(
+        [conv_proj_state[:, 1:], proj_out.reshape(q, 1, 2, gs)], axis=1
+    )
+    return (layer_out, state_out.reshape(head_state.shape), conv_out, conv_proj_out)
+
+
 def solution(mesh):
+    n, nc = mesh.shape["ep"], mesh.shape["tp"]
     placed = (
         P("ep", None),
         P("ep", "tp", None, None),
@@ -234,8 +728,15 @@
         P(("ep", "tp"), None),
         P(),
     )
+
+    def body(*args):
+        seq, width = args[0].shape
+        if width == n * LANES and seq == nc and args[5].shape[1] % LANES == 0:
+            return fused_local(n, nc, *args)
+        return local(*args)
+
     return jax.shard_map(
-        local,
+        body,
         mesh=mesh,
         in_specs=placed,
         out_specs=(

time: 367 us -> 47.2 us (0.13)
  blocking collectives: 194 us -> 0 us
  waiting for transfers between devices: 124 us -> 0 us
  Pallas kernels: 0 us -> 34.5 us
  matrix products: 15.7 us -> 0 us
  between operations: 15.2 us -> 0.65 us
  starting transfers between devices: 8.42 us -> 0 us
  local copies, waits for them, and re-layouts: 2.16 us -> 7.41 us
    unnamed x3 -> x0, waiting for transfers between devices: 124 us -> none
    all_gather x3 -> x0, blocking collectives: 115 us -> none  [the longest x1 41.6 us: local(): lax.all_gather(routes, 'ep', axis=0, tiled=True)]
    unnamed x1 -> x0, blocking collectives: 75.9 us -> none
    pallas_call x0 -> x1, Pallas kernels: none -> 34.5 us  [fused_local(): pl.pallas_call(functools.partial(layer_kernel, n, nc, names, tuple(scratc...]
    dot_general x13 -> x0, matrix products: 15.7 us -> none  [the longest x1 2.84 us: local(): jnp.dot(mixer_rows, lax.all_gather(out_weight, 'ep', axis=1, tiled=True),...]
    all_to_all x1 -> x0, starting transfers between devices: 8.34 us -> none  [local(): lax.all_to_all(normed_in, 'ep', split_axis=1, concat_axis=0, tiled=True)]
    unnamed x43 -> x4, local copies, waits for them, and re-layouts: 0.84 us -> 6.05 us
  transfers between devices with their start and end apart: 3 -> 0, of which waited for: 1 -> 0; matrix products, arithmetic and copies ran while one was open for 4% -> 0% of each run, Pallas kernels for 0% -> 0%
where the time goes in v1:
time: 47.2 us; the launch traced here: 46.6 us
  Pallas kernels  34.5 us (73%)
  local copies, waits for them, and re-layouts  7.41 us (16%)
  other arithmetic  3.97 us (8%)
  between operations  0.65 us (1%)
    pallas_call x1, Pallas kernels, fused_local(): pl.pallas_call(functools.partial(layer_kernel, n, nc, names, tuple(scratc...  34.5 us
    unnamed x4, local copies, waits for them, and re-layouts  6.05 us
    reduce_sum x1, other arithmetic, fused_local(): jnp.sum(conv_state.astype(F32) * conv_kernel[None, :taps - 1], axis=1)  1.36 us
    concatenate x1, other arithmetic, fused_local(): conv_out = jnp.concatenate([conv_state[:, 1:], inner_out[:, None]], axis=1)  1.3 us

profile of v1, /device:TPU:0, one launch (start us, length us, event | category | flops | bytes accessed | tf_op | source)
XLA Modules:
  0.0 46.6 jit_solution(1446103275030841004)
XLA Ops:
  0.6 1.8 %copy.30.refs_19_ = bf16[2048,16]{1,0:T(8,128)(2,1)} copy(bf16[2048,16]{0,1:T(8,128)(2,1)} %param.35) | data formatting | bytes 131072 | tf_op args[9]
  2.5 0.7 %slice.13 = f32[3,2,256]{2,1,0:T(2,128)S(1)} slice(f32[4,2,256]{2,1,0:T(2,128)} %refs_5_.1), slice={[0:3], [0:2], [0:256]} | slice | bytes 12288 | tf_op jit(solution)/shard_map/slice | solution.py:598
  3.2 0.7 %multiply_reduce_fusion.1 = f32[2,2,256]{2,1,0:T(2,128)S(1)} fusion(bf16[2,3,2,256]{3,2,1,0:T(2,128)(2,1)} %param.29, f32[3,2,256]{2,1,0:T(2,128)S(1)} %slice.13), kind=kLoop, calls=%fused_computation.2 | loop fusion | flops 8192 | bytes 16384 | tf_op jit(solution)/shard_map/reduce_sum | solution.py:597
  3.9 0.6 %copy.32 = f32[1,2,2,256]{3,1,2,0:T(2,128)} copy(f32[1,2,2,256]{3,2,1,0:T(2,128)S(1)} %bitcast.24) | data formatting | bytes 8192
  4.5 1.4 %multiply_reduce_fusion.refs_2_ = f32[2,1024]{1,0:T(2,128)} fusion(bf16[2,3,1024]{2,0,1:T(2,128)(2,1)} %param.28, f32[3,1024]{1,0:T(4,128)} %bitcast.22), kind=kLoop, calls=%fused_computation | loop fusion | flops 16384 | bytes 32768 | tf_op jit(solution)/shard_map/reduce_sum | solution.py:596
  5.8 0.0 slice-start
  5.8 0.0 slice-start.1
  5.8 34.5 %shard_map.273 = (bf16[1,2048]{1,0:T(2,128)(2,1)}, f32[2,1024,128]{2,1,0:T(8,128)}, bf16[2,1024]{1,0:T(2,128)(2,1)}, bf16[2,512]{1,0:T(2,128)(2,1)}) custom-call(bf16[2,2048]{1,0:T(2,128)(2,1)} %refs_0_.1, f32[1,2048]{1,0:T(1,128)} %bitcast.26, f32[2,1024]{1,0:T(2,128)} %multiply_reduce_fusion.refs_2_, f32[2,512]{1,0:T(2,128)} %bitcast.23, ...), custom_call_target="tpu_custom_call" | custom-call | tf_op jit(solution)/shard_map/pallas_call | solution.py:684
  40.4 0.0 slice-done
  40.4 1.3 %pad_maximum_fusion = bf16[2,3,1024]{2,0,1:T(2,128)(2,1)} fusion(bf16[2,1,1024]{2,0,1:T(2,128)(2,1)} %bitcast.30, bf16[2,2,1024]{2,0,1:T(2,128)(2,1)S(1)} %slice-done), kind=kLoop, calls=%fused_computation.1 | loop fusion | flops 6144 | bytes 24576 | tf_op jit(solution)/shard_map/concatenate | solution.py:694
  41.7 0.7 %reshape.25 = bf16[2,1,2,256]{3,2,0,1:T(2,128)(2,1)S(1)} reshape(bf16[2,512]{1,0:T(2,128)(2,1)} %get-tuple-element.11) | data formatting | bytes 4096 | tf_op jit(solution)/shard_map/reshape | solution.py:696
  42.3 0.0 slice-done.1
  42.3 0.6 %pad_maximum_fusion.1 = bf16[2,3,2,256]{3,2,1,0:T(2,128)(2,1)} fusion(bf16[2,1,2,256]{3,2,1,0:T(2,128)(2,1)S(1)} %bitcast.25, bf16[2,2,2,256]{3,2,1,0:T(2,128)(2,1)S(1)} %slice-done.1), kind=kLoop, calls=%fused_computation.3 | loop fusion | flops 3072 | bytes 12288 | tf_op jit(solution)/shard_map/concatenate | solution.py:695
  42.9 1.3 %copy.35 = bf16[1,2048]{1,0:T(2,128)(2,1)} copy(bf16[1,2048]{1,0:T(2,128)(2,1)} %get-tuple-element.16) | data formatting | bytes 8192
  44.2 2.3 %copy.36 = f32[2,16,64,128]{3,2,1,0:T(8,128)} copy(f32[2,16,64,128]{3,2,1,0:T(8,128)} %bitcast.21) | data formatting | bytes 2097152
Async XLA Ops:
  5.8 34.5 %slice-start = ((bf16[2,3,1024]{2,0,1:T(2,128)(2,1)}), bf16[2,2,1024]{2,0,1:T(2,128)(2,1)S(1)}, s32[]{:S(2)}) async-start(bf16[2,3,1024]{2,0,1:T(2,128)(2,1)} %param.28), calls=%async_computation | async-start | bytes 16384 | tf_op jit(solution)/shard_map/slice | solution.py:694
  5.8 36.5 %slice-start.1 = ((bf16[2,3,2,256]{3,2,1,0:T(2,128)(2,1)}), bf16[2,2,2,256]{3,2,1,0:T(2,128)(2,1)S(1)}, s32[]{:S(2)}) async-start(bf16[2,3,2,256]{3,2,1,0:T(2,128)(2,1)} %param.29), calls=%async_computation.1 | async-start | bytes 8192 | tf_op jit(solution)/shard_map/slice | solution.py:696

commit v2 on v1

--- a/solution.py
+++ b/solution.py
@@ -353,7 +353,9 @@
     step_load.wait()
     write_proj = dot(own_b, r.write_v[...])[0:q].astype(BF16)
     read_proj = dot(own_b, r.read_v[...])[0:q].astype(BF16)
-    step_raw = dot(own_b, r.step_v[...])[0:q]
+    step_raw = lax.dot_general(
+        own_b, r.step_v[...], (((1,), (1,)), ((), ())), preferred_element_type=F32
+    )[0:q]
 
     take(0, send1, r.recv1, slot1)
     recv1 = r.recv1
@@ -375,12 +377,30 @@
     r.send2[...] = pack2[...].astype(BF16)
     all_to_all(1, r.send2, r.recv2, slot2)
 
-    r.proj_out[:, 0 : groups * state_width] = write_proj
-    r.proj_out[:, groups * state_width :] = read_proj
-    proj_tap = r.conv_proj_kernel[r.conv_proj_kernel.shape[0] - 1]
     gs = groups * state_width
-    write = silu(r.proj_part[:, 0:gs] + write_proj.astype(F32) * proj_tap[0:1])
-    read = silu(r.proj_part[:, gs:] + read_proj.astype(F32) * proj_tap[1:2])
+    taps = r.conv_kernel.shape[0]
+    for s in range(q):
+        fresh = r.fresh
+        fresh[0:1, :] = write_proj[s : s + 1].astype(F32)
+        fresh[1:2, :] = read_proj[s : s + 1].astype(F32)
+        newest = fresh[0:2, :]
+        r.proj_out[s, taps - 2] = newest.astype(BF16)
+        window = newest * r.conv_proj_kernel[taps - 1]
+        for j in range(taps - 1):
+            held = r.conv_proj_state[s, j]
+            if j > 0:
+                r.proj_out[s, j - 1] = held
+            window += held.astype(F32) * r.conv_proj_kernel[j]
+        window = silu(window)
+        r.vectors[s : s + 1, 0:gs] = window[0:1]
+        r.vectors[s : s + 1, gs:] = window[1:2]
+    write, read = r.vectors[0:q, 0:gs], r.vectors[0:q, gs:]
+    inner_part = jnp.zeros((q, half), F32)
+    for j in range(taps - 1):
+        held = r.conv_state[j]
+        if j > 0:
+            r.conv_out[j - 1] = held
+        inner_part += held.astype(F32) * r.conv_kernel[j : j + 1, :]
     pre = step_raw + r.step_bias[...]
     step_size = jnp.maximum(pre, 0.0) + jnp.log1p(jnp.exp(-jnp.abs(pre)))
     decay = jnp.exp(-jnp.exp(r.log_rate[...]) * step_size)
@@ -436,9 +456,7 @@
     r.sum2[...] = total
     gate_proj = lanes_of(r.sum2, 0, q, 2 * chunks, chunks).astype(BF16).astype(F32)
     inner_proj = lanes_of(r.sum2, chunks, q, 2 * chunks, chunks).astype(BF16)
-    last_tap = r.conv_kernel.shape[0] - 1
-    taps = r.conv_kernel[last_tap : last_tap + 1, :]
-    conv_inner = silu(r.inner_part[...] + inner_proj.astype(F32) * taps)
+    conv_inner = silu(inner_part + inner_proj.astype(F32) * r.conv_kernel[taps - 1 : taps, :])
     gated = (carried + direct * conv_inner) * silu(gate_proj)
     normal = []
     for g in range(groups):
@@ -452,7 +470,7 @@
     r.send3[...] = r.pack3[...].astype(BF16)
     all_to_all(2, r.send3, r.recv3, slot3, same=True)
 
-    r.inner_out[...] = inner_proj
+    r.conv_out[taps - 2] = inner_proj
     turn = r.turn
     turn[...] = jnp.zeros_like(turn)
     turn[0:q, :] = decay_rows
@@ -462,13 +480,11 @@
         for k in range(chunks):
             span = slice(k * LANES, (k + 1) * LANES)
             g = k * LANES // group_width
-            r.hs[s, span, :] = (
+            r.state_out[s, span, :] = (
                 columns[span, s : s + 1] * r.hs[s, span, :]
                 + columns[span, q + s : q + s + 1]
                 * write[s : s + 1, g * state_width : (g + 1) * state_width]
             )
-    store = pltpu.make_async_copy(r.hs, r.state_out, r.load_sem.at[len(order)])
-    store.start()
     raw_block = gathered(q)
     out_load.wait()
 
@@ -547,13 +563,23 @@
     summed = jnp.concatenate([r.sum6[j : j + 1, :] for j in range(wide_chunks)], axis=1)
     r.layer_out[...] = (own_row + summed).astype(BF16)
 
-    store.wait()
     drain(r.send_sem.at[0], send1, (n - 1) * slot1)
     drain(r.send_sem.at[1], r.send2, (n - 1) * slot2)
     drain(r.send_sem.at[2], r.recv3, (n - 1) * slot3)
     swap.wait_send()
     drain(r.send_sem.at[4], r.recv5, (n - 1) * rows)
     drain(r.send_sem.at[5], r.send6, (n * nc - 1) * slot6)
+
+
+def store_kernel(*refs):
+    count = len(refs) // 2
+    copies = [
+        pltpu.make_async_copy(refs[i], refs[count + i], refs[-1].at[i]) for i in range(count)
+    ]
+    for copy in copies:
+        copy.start()
+    for copy in copies:
+        copy.wait()
 
 
 def fused_local(
@@ -593,15 +619,11 @@
     gs = write_weight.shape[1]
     heads, state_width = head_state.shape[1], head_state.shape[3]
     taps = conv_kernel.shape[0]
-    inner_part = jnp.sum(conv_state.astype(F32) * conv_kernel[None, : taps - 1], axis=1)
-    proj_part = jnp.sum(
-        conv_proj_state.astype(F32) * conv_proj_kernel[None, : taps - 1], axis=1
-    ).reshape(q, 2 * gs)
     small_in = dict(
         tokens=tokens,
         first_gain=first_gain[None],
-        inner_part=inner_part,
-        proj_part=proj_part,
+        conv_state=jnp.transpose(conv_state, (1, 0, 2)),
+        conv_proj_state=conv_proj_state,
         conv_kernel=conv_kernel,
         conv_proj_kernel=conv_proj_kernel,
         step_bias=step_bias[None],
@@ -619,7 +641,7 @@
         inner_weight=inner_weight,
         write_weight=write_weight,
         read_weight=read_weight,
-        step_weight=step_weight,
+        step_weight=step_weight.T,
         out_weight=out_weight,
         expert_gate=expert_gate[0],
         expert_up=expert_up[0],
@@ -627,22 +649,22 @@
         dense_up=dense_up,
         dense_down=dense_down,
     )
+    vmem = pltpu.VMEM
     outs = dict(
-        layer_out=jax.ShapeDtypeStruct((q // nc, width), BF16),
-        state_out=jax.ShapeDtypeStruct((q, half, state_width), F32),
-        inner_out=jax.ShapeDtypeStruct((q, half), BF16),
-        proj_out=jax.ShapeDtypeStruct((q, 2 * gs), BF16),
+        layer_out=vmem((q // nc, width), BF16),
+        state_out=vmem((q, half, state_width), F32),
+        conv_out=vmem((taps - 1, q, half), BF16),
+        proj_out=vmem((q, taps - 1, 2, gs), BF16),
     )
     slot1 = -(-4 * q // 8) * 8
     slot2, slot3, slot6 = 2 * q * chunks, q * chunks, wide_chunks
     small_rows = -(-(2 * q + 1) // 8) * 8
-    vmem = pltpu.VMEM
     scratch = dict(
         gate_v=vmem(gate_weight.shape, BF16),
         inner_v=vmem(inner_weight.shape, BF16),
         write_v=vmem(write_weight.shape, BF16),
         read_v=vmem(read_weight.shape, BF16),
-        step_v=vmem(step_weight.shape, BF16),
+        step_v=vmem(step_weight.shape[::-1], BF16),
         hs=vmem((q, half, state_width), F32),
         out_v=vmem(out_weight.shape, BF16),
         eg_v=vmem(expert_gate.shape[1:], BF16),
@@ -657,6 +679,8 @@
         send2=vmem((n * slot2, LANES), BF16),
         recv2=vmem((n * slot2, LANES), BF16),
         sum2=vmem((slot2, LANES), F32),
+        fresh=vmem((8, gs), F32),
+        vectors=vmem((8, 2 * gs), F32),
         small=vmem((small_rows, heads), F32),
         reads=vmem((8, gs), F32),
         old_read=vmem((8, half), F32),
@@ -674,28 +698,36 @@
         send6=vmem((rows * slot6, LANES), BF16),
         recv6=vmem((n * nc * slot6, LANES), BF16),
         sum6=vmem((slot6, LANES), F32),
-        load_sem=pltpu.SemaphoreType.DMA((13,)),
+        load_sem=pltpu.SemaphoreType.DMA((12,)),
         send_sem=pltpu.SemaphoreType.DMA((6,)),
         recv_sem=pltpu.SemaphoreType.DMA((6,)),
     )
     in_vmem = pl.BlockSpec(memory_space=pltpu.VMEM)
     anywhere = pl.BlockSpec(memory_space=pl.ANY)
     names = tuple(small_in) + tuple(big_in) + tuple(outs)
-    layer_out, state_out, inner_out, proj_out = pl.pallas_call(
+    results = pl.pallas_call(
         functools.partial(layer_kernel, n, nc, names, tuple(scratch)),
         out_shape=tuple(outs.values()),
         in_specs=[in_vmem] * len(small_in) + [anywhere] * len(big_in),
-        out_specs=(in_vmem, anywhere, in_vmem, in_vmem),
+        out_specs=(in_vmem,) * len(outs),
         scratch_shapes=list(scratch.values()),
         compiler_params=pltpu.CompilerParams(
             collective_id=0, has_side_effects=True, vmem_limit_bytes=60 * 1024 * 1024
         ),
     )(*small_in.values(), *big_in.values())
-    conv_out = jnp.concatenate([conv_state[:, 1:], inner_out[:, None]], axis=1)
-    conv_proj_out = jnp.concatenate(
-        [conv_proj_state[:, 1:], proj_out.reshape(q, 1, 2, gs)], axis=1
-    )
-    return (layer_out, state_out.reshape(head_state.shape), conv_out, conv_proj_out)
+    layer_out, state_out, conv_out, proj_out = pl.pallas_call(
+        store_kernel,
+        out_shape=tuple(jax.ShapeDtypeStruct(a.shape, a.dtype) for a in results),
+        in_specs=[in_vmem] * len(results),
+        out_specs=(anywhere,) * len(results),
+        scratch_shapes=[pltpu.SemaphoreType.DMA((len(results),))],
+    )(*[pltpu.with_memory_space_constraint(a, pltpu.VMEM) for a in results])
+    return (
+        layer_out,
+        state_out.reshape(head_state.shape),
+        jnp.transpose(conv_out, (1, 0, 2)),
+        proj_out,
+    )
 
 
 def solution(mesh):

time: 47.2 us -> 35.8 us (0.76)
  local copies, waits for them, and re-layouts: 7.41 us -> 0 us
  other arithmetic: 3.97 us -> 0 us
  Pallas kernels: 34.5 us -> 35 us
    unnamed x4 -> x0, local copies, waits for them, and re-layouts: 6.05 us -> none
    reduce_sum x2 -> x0, other arithmetic: 2.06 us -> none  [the longest x1 1.36 us: fused_local(): jnp.sum(conv_state.astype(F32) * conv_kernel[None, :taps - 1], axis=1)]
    concatenate x2 -> x0, other arithmetic: 1.9 us -> none  [the longest x1 1.3 us: fused_local(): conv_out = jnp.concatenate([conv_state[:, 1:], inner_out[:, None]], axis=1)]
    pallas_call x0 -> x1, Pallas kernels: none -> 1.02 us  [fused_local(): pl.pallas_call(store_kernel, out_shape=tuple((jax.ShapeDtypeStruct(a.shap...]
    slice x5 -> x0, local copies, waits for them, and re-layouts: 0.7 us -> none  [the longest x1 0.69 us: fused_local(): conv_proj_kernel[None, :taps - 1]]
    reshape x1 -> x0, local copies, waits for them, and re-layouts: 0.66 us -> none  [fused_local(): proj_out.reshape(q, 1, 2, gs)]
    pallas_call x1, Pallas kernels: 34.5 us -> 33.9 us  [fused_local(): pl.pallas_call(functools.partial(layer_kernel, n, nc, names, tuple(scratc...]
where the time goes in v2:
time: 35.8 us; the launch traced here: 35.6 us
  Pallas kernels  35 us (98%)
  between operations  0.65 us (2%)
    pallas_call x1, Pallas kernels, fused_local(): pl.pallas_call(functools.partial(layer_kernel, n, nc, names, tuple(scratc...  33.9 us
    pallas_call x1, Pallas kernels, fused_local(): pl.pallas_call(store_kernel, out_shape=tuple((jax.ShapeDtypeStruct(a.shap...  1.02 us

profile of v2, /device:TPU:0, one launch (start us, length us, event | category | flops | bytes accessed | tf_op | source)
XLA Modules:
  0.0 35.6 jit_solution(15438149586529502918)
XLA Ops:
  0.6 33.9 %shard_map.273 = (bf16[1,2048]{1,0:T(2,128)(2,1)S(1)}, f32[2,1024,128]{2,1,0:T(8,128)S(1)}, bf16[3,2,1024]{2,1,0:T(2,128)(2,1)S(1)}, bf16[2,3,2,256]{3,2,1,0:T(2,128)(2,1)S(1)}) custom-call(bf16[2,2048]{1,0:T(2,128)(2,1)} %refs_0_.1, f32[1,2048]{1,0:T(1,128)} %bitcast.21, bf16[3,2,1024]{2,1,0:T(2,128)(2,1)} %bitcast.20, bf16[2,3,2,256]{3,2,1,0:T(2,128)(2,1)} %refs_3_.1, ...), custom_call_target="tpu_custom_call" | custom-call | tf_op jit(solution)/shard_map/pallas_call | solution.py:708
  34.6 1.0 %shard_map.274 = (bf16[1,2048]{1,0:T(2,128)(2,1)}, f32[2,1024,128]{2,1,0:T(8,128)}, bf16[3,2,1024]{2,1,0:T(2,128)(2,1)}, bf16[2,3,2,256]{3,2,1,0:T(2,128)(2,1)}) custom-call(bf16[1,2048]{1,0:T(2,128)(2,1)S(1)} %get-tuple-element.12.refs_0_, f32[2,1024,128]{2,1,0:T(8,128)S(1)} %get-tuple-element.13.refs_1_, ...), custom_call_target="tpu_custom_call" | custom-call | tf_op jit(solution)/shard_map/pallas_call | solution.py:718

commit v3 on v2

--- a/solution.py
+++ b/solution.py
@@ -233,20 +233,23 @@
 def layer_kernel(
     n,
     nc,
+    small_names,
     names,
     scratch_names,
     *refs,
 ):
-    r = types.SimpleNamespace(**dict(zip(names + scratch_names, refs)))
+    small_count = len(small_names)
+    small_src, refs = refs[:small_count], refs[small_count:]
+    r = types.SimpleNamespace(**dict(zip(names + scratch_names + small_names, refs)))
+    small_dst = refs[len(refs) - small_count :]
     me = lax.axis_index("ep")
     core = lax.axis_index("tp")
-    q = r.tokens.shape[0]
-    width = r.tokens.shape[1]
+    q, width = r.tokens.shape
     half = r.gate_v.shape[1]
     chunks = half // LANES
     wide_chunks = width // LANES
     rows = n * q
-    slot1 = r.send1.shape[0] // n
+    slot0 = r.send0.shape[0] // n
     slot2 = 2 * q * chunks
     slot3 = q * chunks
     slot6 = wide_chunks
@@ -268,6 +271,12 @@
 
     lax.fori_loop(1, n * nc, greet, 0)
 
+    small_loads = [
+        pltpu.make_async_copy(src, dst, r.small_sem.at[i])
+        for i, (src, dst) in enumerate(zip(small_src, small_dst))
+    ]
+    for load in small_loads:
+        load.start()
     order = (
         (r.gate_weight, r.gate_v),
         (r.inner_weight, r.inner_v),
@@ -285,8 +294,6 @@
     loads = [
         pltpu.make_async_copy(src, dst, r.load_sem.at[i]) for i, (src, dst) in enumerate(order)
     ]
-    for load in loads:
-        load.start()
     (
         gate_load,
         inner_load,
@@ -301,22 +308,38 @@
         expert_down_load,
         dense_down_load,
     ) = loads
+    gate_load.start()
+    inner_load.start()
+
+    def partner(step):
+        if n & (n - 1):
+            return lax.rem(me + step, n)
+        other, bit = 0, 1
+        while bit < n:
+            digit = lax.rem(me // bit, 2)
+            other += bit * (1 - digit if step & bit else digit)
+            bit *= 2
+        return other
+
+    partners = [partner(step) for step in range(n)]
+
+    def send_to(phase, src, dst, peer, peer_core):
+        pltpu.make_async_remote_copy(
+            src_ref=src,
+            dst_ref=dst,
+            send_sem=r.send_sem.at[phase],
+            recv_sem=r.recv_sem.at[phase],
+            device_id=(peer, peer_core),
+            device_id_type=MESH,
+        ).start()
 
     def all_to_all(phase, send, recv, slot, same=False):
-        def one(step, _):
-            peer = lax.rem(me + step, n)
+        for step in reversed(range(1, n)):
+            peer = partners[step]
             src = send if same else send.at[pl.ds(pl.multiple_of(peer * slot, slot), slot)]
-            pltpu.make_async_remote_copy(
-                src_ref=src,
-                dst_ref=recv.at[pl.ds(pl.multiple_of(me * slot, slot), slot)],
-                send_sem=r.send_sem.at[phase],
-                recv_sem=r.recv_sem.at[phase],
-                device_id=(peer, core),
-                device_id_type=MESH,
-            ).start()
-            return 0
-
-        lax.fori_loop(1, n, one, 0)
+            send_to(
+                phase, src, recv.at[pl.ds(pl.multiple_of(me * slot, slot), slot)], peer, core
+            )
 
     def drain(sem, buffer, count):
         part = buffer.at[pl.ds(0, count)]
@@ -327,45 +350,38 @@
         mine = pl.ds(pl.multiple_of(me * slot, slot), slot)
         recv[mine, :] = send[...] if same else send[mine, :]
 
+    for load in small_loads:
+        load.wait()
     x = r.tokens[...].astype(F32)
     normed = rms_scale(x, r.first_gain[...]).astype(BF16).astype(F32)
-    send1 = r.send1
-    send1[...] = jnp.zeros_like(send1)
+    for e in range(n):
+        r.send1[e] = normed[:, e * LANES : (e + 1) * LANES]
+    pl.semaphore_wait(barrier, n * nc - 1)
+    for step in reversed(range(1, n)):
+        send_to(0, r.send1.at[partners[step]], r.recv1.at[me], partners[step], core)
+    for load in (write_load, read_load, step_load, state_load, out_load):
+        load.start()
+    send0 = r.send0
+    send0[...] = jnp.zeros_like(send0)
     chosen = r.routes[...].astype(F32)
     scores = r.route_logits[...].astype(F32)
     for e in range(n):
-        at, cut = e * slot1, slice(e * LANES, (e + 1) * LANES)
-        send1[at : at + q, :] = normed[:, cut]
-        send1[at + q : at + 2 * q, :] = x[:, cut]
-        send1[at + 2 * q : at + 3 * q, 0:topk] = chosen
-        send1[at + 3 * q : at + 4 * q, 0:topk] = scores
-    pl.semaphore_wait(barrier, n * nc - 1)
-    all_to_all(0, send1, r.recv1, slot1)
-
+        at, cut = e * slot0, slice(e * LANES, (e + 1) * LANES)
+        send0[at : at + q, :] = x[:, cut]
+        send0[at + q : at + 2 * q, 0:topk] = chosen
+        send0[at + 2 * q : at + 3 * q, 0:topk] = scores
+    all_to_all(6, send0, r.recv0, slot0)
     own = r.own_rows
     own[...] = jnp.zeros_like(own)
     own[0:q, :] = normed
     own_b = own[...].astype(BF16)
     gate_load.wait()
     inner_load.wait()
-    write_load.wait()
-    read_load.wait()
-    step_load.wait()
-    write_proj = dot(own_b, r.write_v[...])[0:q].astype(BF16)
-    read_proj = dot(own_b, r.read_v[...])[0:q].astype(BF16)
-    step_raw = lax.dot_general(
-        own_b, r.step_v[...], (((1,), (1,)), ((), ())), preferred_element_type=F32
-    )[0:q]
-
-    take(0, send1, r.recv1, slot1)
-    recv1 = r.recv1
-
-    def gathered(offset):
-        return jnp.concatenate(
-            [recv1[pl.ds(offset + s, n, stride=slot1), :] for s in range(q)], axis=0
-        )
-
-    features = gathered(0).astype(BF16)
+
+    drain(r.recv_sem.at[0], r.recv1, n - 1)
+    r.recv1[me] = r.send1[me]
+
+    features = jnp.concatenate([r.recv1[:, s, :] for s in range(q)], axis=0).astype(BF16)
     pack2 = r.pack2
     for g, weight in enumerate((r.gate_v, r.inner_v)):
         part = dot(features, weight[...])
@@ -377,6 +393,16 @@
     r.send2[...] = pack2[...].astype(BF16)
     all_to_all(1, r.send2, r.recv2, slot2)
 
+    for load in loads[7:]:
+        load.start()
+    write_load.wait()
+    read_load.wait()
+    step_load.wait()
+    write_proj = dot(own_b, r.write_v[...])[0:q].astype(BF16)
+    read_proj = dot(own_b, r.read_v[...])[0:q].astype(BF16)
+    step_raw = lax.dot_general(
+        own_b, r.step_v[...], (((1,), (1,)), ((), ())), preferred_element_type=F32
+    )[0:q]
     gs = groups * state_width
     taps = r.conv_kernel.shape[0]
     for s in range(q):
@@ -441,14 +467,6 @@
     carried = decay_rows * old_read[0:q, :]
     direct = step_rows * jnp.concatenate(write_read, axis=1) + skip_rows
 
-    all_routes, all_scores = gathered(2 * q), gathered(3 * q)
-    real = lax.broadcasted_iota(jnp.int32, (rows, LANES), 1) < topk
-    top = jnp.max(jnp.where(real, all_scores, -jnp.inf), axis=1, keepdims=True)
-    raised = jnp.where(real, jnp.exp(jnp.where(real, all_scores - top, 0.0)), 0.0)
-    gates = raised / jnp.sum(raised, axis=1, keepdims=True)
-    hits = real & (all_routes == me.astype(F32))
-    row_weight = jnp.sum(jnp.where(hits, gates, 0.0), axis=1, keepdims=True)
-
     take(1, r.send2, r.recv2, slot2)
     total = r.recv2[0:slot2, :].astype(F32)
     for e in range(1, n):
@@ -485,7 +503,21 @@
                 + columns[span, q + s : q + s + 1]
                 * write[s : s + 1, g * state_width : (g + 1) * state_width]
             )
-    raw_block = gathered(q)
+    take(6, send0, r.recv0, slot0)
+
+    def gathered(offset):
+        return jnp.concatenate(
+            [r.recv0[pl.ds(offset + s, n, stride=slot0), :] for s in range(q)], axis=0
+        )
+
+    raw_block = gathered(0)
+    all_routes, all_scores = gathered(q), gathered(2 * q)
+    real = lax.broadcasted_iota(jnp.int32, (rows, LANES), 1) < topk
+    top = jnp.max(jnp.where(real, all_scores, -jnp.inf), axis=1, keepdims=True)
+    raised = jnp.where(real, jnp.exp(jnp.where(real, all_scores - top, 0.0)), 0.0)
+    gates = raised / jnp.sum(raised, axis=1, keepdims=True)
+    hits = real & (all_routes == me.astype(F32))
+    row_weight = jnp.sum(jnp.where(hits, gates, 0.0), axis=1, keepdims=True)
     out_load.wait()
 
     take(2, r.send3, r.recv3, slot3, same=True)
@@ -535,22 +567,12 @@
     r.send6[...] = r.pack6[...].astype(BF16)
     mine = me * nc + core
 
-    def one(step, _):
-        other = lax.rem(mine + step, n * nc)
-        peer, peer_core = other // nc, lax.rem(other, nc)
-        pltpu.make_async_remote_copy(
-            src_ref=r.send6.at[
-                pl.ds(pl.multiple_of((peer_core * n + peer) * slot6, slot6), slot6)
-            ],
-            dst_ref=r.recv6.at[pl.ds(pl.multiple_of(mine * slot6, slot6), slot6)],
-            send_sem=r.send_sem.at[5],
-            recv_sem=r.recv_sem.at[5],
-            device_id=(peer, peer_core),
-            device_id_type=MESH,
-        ).start()
-        return 0
-
-    lax.fori_loop(1, n * nc, one, 0)
+    into = r.recv6.at[pl.ds(pl.multiple_of(mine * slot6, slot6), slot6)]
+    for step in reversed(range(n)):
+        for turn_core in range(1 if step == 0 else 0, nc):
+            peer, peer_core = partners[step], lax.rem(core + turn_core, nc)
+            row = pl.multiple_of((peer_core * n + peer) * slot6, slot6)
+            send_to(5, r.send6.at[pl.ds(row, slot6)], into, peer, peer_core)
     own_row = r.hidden[pl.ds(core * n + me, 1), :]
     drain(r.recv_sem.at[5], r.recv6, (n * nc - 1) * slot6)
     r.recv6[pl.ds(pl.multiple_of(mine * slot6, slot6), slot6), :] = r.send6[
@@ -563,7 +585,8 @@
     summed = jnp.concatenate([r.sum6[j : j + 1, :] for j in range(wide_chunks)], axis=1)
     r.layer_out[...] = (own_row + summed).astype(BF16)
 
-    drain(r.send_sem.at[0], send1, (n - 1) * slot1)
+    drain(r.send_sem.at[0], r.send1, n - 1)
+    drain(r.send_sem.at[6], send0, (n - 1) * slot0)
     drain(r.send_sem.at[1], r.send2, (n - 1) * slot2)
     drain(r.send_sem.at[2], r.recv3, (n - 1) * slot3)
     swap.wait_send()
@@ -656,7 +679,7 @@
         conv_out=vmem((taps - 1, q, half), BF16),
         proj_out=vmem((q, taps - 1, 2, gs), BF16),
     )
-    slot1 = -(-4 * q // 8) * 8
+    slot0 = -(-3 * q // 8) * 8
     slot2, slot3, slot6 = 2 * q * chunks, q * chunks, wide_chunks
     small_rows = -(-(2 * q + 1) // 8) * 8
     scratch = dict(
@@ -672,8 +695,10 @@
         du_v=vmem(dense_up.shape, BF16),
         ed_v=vmem(expert_down.shape[1:], BF16),
         dd_v=vmem(dense_down.shape, BF16),
-        send1=vmem((n * slot1, LANES), F32),
-        recv1=vmem((n * slot1, LANES), F32),
+        send0=vmem((n * slot0, LANES), F32),
+        recv0=vmem((n * slot0, LANES), F32),
+        send1=vmem((n, q, LANES), F32),
+        recv1=vmem((n, q, LANES), F32),
         own_rows=vmem((16, width), F32),
         pack2=vmem((n * slot2, LANES), F32),
         send2=vmem((n * slot2, LANES), BF16),
@@ -699,18 +724,20 @@
         recv6=vmem((n * nc * slot6, LANES), BF16),
         sum6=vmem((slot6, LANES), F32),
         load_sem=pltpu.SemaphoreType.DMA((12,)),
-        send_sem=pltpu.SemaphoreType.DMA((6,)),
-        recv_sem=pltpu.SemaphoreType.DMA((6,)),
+        small_sem=pltpu.SemaphoreType.DMA((len(small_in),)),
+        send_sem=pltpu.SemaphoreType.DMA((7,)),
+        recv_sem=pltpu.SemaphoreType.DMA((7,)),
     )
     in_vmem = pl.BlockSpec(memory_space=pltpu.VMEM)
     anywhere = pl.BlockSpec(memory_space=pl.ANY)
-    names = tuple(small_in) + tuple(big_in) + tuple(outs)
+    names = tuple(big_in) + tuple(outs)
     results = pl.pallas_call(
-        functools.partial(layer_kernel, n, nc, names, tuple(scratch)),
+        functools.partial(layer_kernel, n, nc, tuple(small_in), names, tuple(scratch)),
         out_shape=tuple(outs.values()),
-        in_specs=[in_vmem] * len(small_in) + [anywhere] * len(big_in),
+        in_specs=[anywhere] * (len(small_in) + len(big_in)),
         out_specs=(in_vmem,) * len(outs),
-        scratch_shapes=list(scratch.values()),
+        scratch_shapes=list(scratch.values())
+        + [vmem(a.shape, a.dtype) for a in small_in.values()],
         compiler_params=pltpu.CompilerParams(
             collective_id=0, has_side_effects=True, vmem_limit_bytes=60 * 1024 * 1024
         ),

time: 35.8 us -> 35.2 us (0.983)
  Pallas kernels: 35 us -> 34.3 us
    pallas_call x1, Pallas kernels: 33.9 us -> 33.3 us  [fused_local(): pl.pallas_call(functools.partial(layer_kernel, n, nc, tuple(small_in), na...]
where the time goes in v3:
time: 35.2 us; the launch traced here: 35 us
  Pallas kernels  34.3 us (97%)
  between operations  0.65 us (2%)
    pallas_call x1, Pallas kernels, fused_local(): pl.pallas_call(functools.partial(layer_kernel, n, nc, tuple(small_in), na...  33.3 us
    pallas_call x1, Pallas kernels, fused_local(): pl.pallas_call(store_kernel, out_shape=tuple((jax.ShapeDtypeStruct(a.shap...  1.02 us

profile of v3, /device:TPU:0, one launch (start us, length us, event | category | flops | bytes accessed | tf_op | source)
XLA Modules:
  0.0 35.0 jit_solution(6515813707839979910)
XLA Ops:
  0.6 33.3 %shard_map.273 = (bf16[1,2048]{1,0:T(2,128)(2,1)S(1)}, f32[2,1024,128]{2,1,0:T(8,128)S(1)}, bf16[3,2,1024]{2,1,0:T(2,128)(2,1)S(1)}, bf16[2,3,2,256]{3,2,1,0:T(2,128)(2,1)S(1)}) custom-call(bf16[2,2048]{1,0:T(2,128)(2,1)} %refs_0_.1, f32[1,2048]{1,0:T(1,128)} %bitcast.21, bf16[3,2,1024]{2,1,0:T(2,128)(2,1)} %bitcast.20, bf16[2,3,2,256]{3,2,1,0:T(2,128)(2,1)} %refs_3_.1, ...), custom_call_target="tpu_custom_call" | custom-call | tf_op jit(solution)/shard_map/pallas_call | solution.py:734
  33.9 1.0 %shard_map.274 = (bf16[1,2048]{1,0:T(2,128)(2,1)}, f32[2,1024,128]{2,1,0:T(8,128)}, bf16[3,2,1024]{2,1,0:T(2,128)(2,1)}, bf16[2,3,2,256]{3,2,1,0:T(2,128)(2,1)}) custom-call(bf16[1,2048]{1,0:T(2,128)(2,1)S(1)} %get-tuple-element.12.refs_0_, f32[2,1024,128]{2,1,0:T(8,128)S(1)} %get-tuple-element.13.refs_1_, ...), custom_call_target="tpu_custom_call" | custom-call | tf_op jit(solution)/shard_map/pallas_call | solution.py:745
